TPU v7x, 32 devices: a whole 2x2x4 slice. The times are simulated.
32 devices in a mesh: sp: 8 (over z, x), tp: 4 (over y, core).
Axes of the slice: x: 2, y: 2, z: 4, core: 2. Of those that a mesh axis runs over, the one named last changes fastest.
Arguments:
- cotangent: bfloat16 [2048, 2048], P('sp'), may hold values from -6 to 6
- route_ids: int32 [2048, 2], P('sp'), may hold values from 0 to 7, all different within a row; in each aligned block of 256 rows (0 to 255, 256 to 511, ...) at most 128 rows name the same one
- route_weights: float32 [2048, 2], P('sp'), may hold values from 0.2 to 1
- expert_inputs: bfloat16 [8, 1024, 2048], P('sp'), may hold values from -6 to 6
- gate_weight: bfloat16 [8, 2048, 1024], P('sp', None, 'tp'), may hold values from -0.125 to 0.125
- up_weight: bfloat16 [8, 2048, 1024], P('sp', None, 'tp'), may hold values from -0.125 to 0.125
- down_weight: bfloat16 [8, 1024, 2048], P('sp', 'tp'), may hold values from -0.1875 to 0.1875
- out_weight: bfloat16 [2048, 512], P(None, 'tp'), may hold values from -0.25 to 0.25
- gate_in: bfloat16 [2048, 512], P('sp', 'tp'), may hold values from -6 to 6
- conv_sum: bfloat16 [2048, 512], P('sp', 'tp'), may hold values from -6 to 6
- conv_c: bfloat16 [2048, 512], P('sp', 'tp'), may hold values from -6 to 6
- conv_v: bfloat16 [2048, 512], P('sp', 'tp'), may hold values from -6 to 6
- conv_taps: float32 [3, 512], P(None, 'tp'), may hold values from -3 to 3
Outputs:
- grad_input: bfloat16 [2048, 2048], P('sp', 'tp')
- grad_gate: bfloat16 [8, 2048, 1024], P('sp', None, 'tp')
- grad_up: bfloat16 [8, 2048, 1024], P('sp', None, 'tp')
- grad_down: bfloat16 [8, 1024, 2048], P('sp', 'tp')
- grad_out_weight: float32 [2048, 512], P('sp', 'tp')
- grad_gate_in: bfloat16 [2048, 512], P('sp', 'tp')
- grad_conv_c: bfloat16 [2048, 512], P('sp', 'tp')
- grad_conv_v: bfloat16 [2048, 512], P('sp', 'tp')
Inputs may be any that keep to these rules, and one draw needn't show every extreme that they name: `route_ids`: the 2 experts of a token differ. Among the 256 tokens of one index of sp no expert is named more than 128 times, and in every draw some expert is named exactly 128 times by the tokens of some index of sp.
All inputs are finite; a program needn't handle non-finite values.
Results may differ from a plain program's by a relative error of at most 0.012.
Values may be sent and summed in bfloat16 or wider, within the bound.
A program may use at most 128 MiB of HBM per device.

v0:
```python
import functools

import jax
import jax.numpy as jnp
from jax import lax
from jax.experimental import pallas as pl
from jax.experimental.pallas import tpu as pltpu
from jax.sharding import PartitionSpec as P

F32 = jnp.float32
BF16 = jnp.bfloat16
NT = (((1,), (1,)), ((), ()))
TN = (((0,), (0,)), ((), ()))


def mm(a, b, dims=(((1,), (0,)), ((), ()))):
    return lax.dot_general(a, b, dims, preferred_element_type=F32)


def kernel(
    n,
    tp,
    ids_ref,
    wts_ref,
    cot_ref,
    x_hbm,
    wg_hbm,
    wu_hbm,
    wd_hbm,
    ow_ref,
    gin_ref,
    csum_ref,
    cc_ref,
    cv_ref,
    taps_ref,
    gi_hbm,
    gg_hbm,
    gu_hbm,
    gd_hbm,
    gow_out,
    ggi_out,
    gcc_out,
    gcv_out,
    x_v,
    wg_v,
    wu_v,
    wd_v,
    sel_v,
    sent_v,
    pair_v,
    routed_v,
    pre_g,
    pre_u,
    hid_v,
    gpg_v,
    gpu_v,
    part_v,
    core_v,
    ysend_v,
    yrecv_v,
    back_v,
    ret_v,
    mid_v,
    term_v,
    terms_v,
    ext_v,
    halo_v,
    gg_v,
    gu_v,
    gd_v,
    load_sem,
    save_sem,
    out_s,
    out_r,
    pair_s,
    pair_r,
    agy_s,
    agy_r,
    agd_s,
    agd_r,
    fwd_s,
    fwd_r,
    core_s,
    core_r,
    y_s,
    y_r,
    ret_s,
    ret_r,
    mid_s,
    mid_r,
    term_s,
    term_r,
    halo_s,
    halo_r,
):
    me = lax.axis_index("sp")
    q = lax.axis_index("tp")
    qd = q + 1 - 2 * (q % 2)
    qy = (q + tp // 2) % tp
    qdy = (qd + tp // 2) % tp
    tokens, width = cot_ref.shape
    slots = x_v.shape[0]
    cap = slots // n
    dq = width // tp
    du = dq // 2
    top = ids_ref.shape[0]

    loads = [
        pltpu.make_async_copy(src.at[0], dst, load_sem.at[i])
        for i, (src, dst) in enumerate(
            ((x_hbm, x_v), (wg_hbm, wg_v), (wu_hbm, wu_v), (wd_hbm, wd_v))
        )
    ]
    for load in loads:
        load.start()

    barrier = pltpu.get_barrier_semaphore()

    def greet(i, carry):
        pl.semaphore_signal(
            barrier, inc=1, device_id=((me + i) % n, q), device_id_type=pl.DeviceIdType.MESH
        )
        return carry

    lax.fori_loop(1, n, greet, 0)
    for other in (qd, qy):
        pl.semaphore_signal(
            barrier, inc=1, device_id=(me, other), device_id_type=pl.DeviceIdType.MESH
        )

    def rows(block):
        return pl.ds(pl.multiple_of(block * cap, cap), cap)

    def unit(part, side):
        return pl.ds(pl.multiple_of((part + side * tp) * du, du), du)

    def gathered(ref, part):
        return jnp.concatenate([ref[:, unit(part, 0)], ref[:, unit(part, 1)]], axis=1)

    def remote(src, dst, ssem, rsem, sp_id, tp_id):
        return pltpu.make_async_remote_copy(
            src_ref=src,
            dst_ref=dst,
            send_sem=ssem,
            recv_sem=rsem,
            device_id=(sp_id, tp_id),
            device_id_type=pl.DeviceIdType.MESH,
        )

    half = n // 2
    pairs = half // 2
    side, low = me // half, me % half
    pair, member = low // 2, low % 2

    twin = n - 1

    def step(p):
        far = (p == 1) | ((p >= 3) & (p < half + 2))
        across = jnp.where(far, 1, 0)
        late = jnp.where(p < 3, p, jnp.where(p == twin, 1, p - half + 1))
        turn = jnp.where(far, jnp.where(p == 1, 0, p - 2), late)
        return (side + across) % 2 * half, turn // 2, turn % 2

    def to(i):
        base, hop, swap = step(i)
        return base + (pair + hop) % pairs * 2 + (member + swap) % 2

    def source(i):
        base, hop, swap = step(i)
        return base + (pair - hop + pairs) % pairs * 2 + (member + swap) % 2

    def c_out(i):
        return remote(
            sent_v.at[rows(to(i))], routed_v.at[q, rows(me)], out_s.at[i], out_r.at[i], to(i), q
        )

    def c_pair():
        return remote(pair_v, routed_v.at[qy, rows(me)], pair_s, pair_r, to(twin), q)

    def c_agy(i):
        block = routed_v.at[q, rows(source(i))]
        return remote(block, block, agy_s.at[i], agy_r.at[i], me, qy)

    def c_agd(i):
        block = routed_v.at[q, rows(source(i))]
        return remote(block, block, agd_s.at[i], agd_r.at[i], me, qd)

    def c_fwd(i):
        block = routed_v.at[qy, rows(source(i))]
        return remote(block, block, fwd_s.at[i], fwd_r.at[i], me, qd)

    def c_core(i, h):
        return remote(
            part_v.at[(qd, qdy)[h], rows(source(i))],
            core_v.at[h, rows(source(i))],
            core_s.at[h, i],
            core_r.at[h, i],
            me,
            qd,
        )

    def c_y(i):
        block = rows(source(i))
        return remote(ysend_v.at[block], yrecv_v.at[block], y_s.at[i], y_r.at[i], me, qy)

    def c_ret(i):
        return remote(
            back_v.at[rows(source(i))], ret_v.at[rows(me)], ret_s.at[i], ret_r.at[i], source(i), q
        )

    ids = ids_ref[...]
    experts = n
    e_iota = lax.broadcasted_iota(jnp.int32, (experts, tokens), 0)
    hits = [e_iota == ids[k : k + 1, :] for k in range(top)]
    named = hits[0].astype(F32)
    for k in range(1, top):
        named = named + hits[k].astype(F32)
    earlier = (
        lax.broadcasted_iota(jnp.int32, (tokens, tokens), 0)
        < lax.broadcasted_iota(jnp.int32, (tokens, tokens), 1)
    ).astype(F32).astype(BF16)
    before = mm(named.astype(BF16), earlier)
    place = [
        jnp.sum(jnp.where(hits[k], before, 0.0), axis=0, keepdims=True)
        + ids[k : k + 1, :].astype(F32) * cap
        for k in range(top)
    ]
    slot_iota = lax.broadcasted_iota(jnp.int32, (cap, tokens), 0)

    def select(block):
        slot = (slot_iota + block * cap).astype(F32)
        mask = jnp.zeros((cap, tokens), F32)
        weight = jnp.zeros((cap, tokens), F32)
        for k in range(top):
            same = slot == place[k]
            mask = jnp.where(same, 1.0, mask)
            weight = jnp.where(same, wts_ref[k : k + 1, :], weight)
        mask = mask.astype(BF16)
        sel_v[rows(block), :] = mask
        return mask, jnp.sum(weight, axis=1, keepdims=True)

    pl.semaphore_wait(barrier, n - 1 + 2)

    def build(i, carry):
        mask, weight = select(to(i))
        sent_v[rows(to(i)), :] = (weight * mm(mask, gathered(cot_ref, q))).astype(BF16)
        c_out(i).start()

        @pl.when(i == twin)
        def _():
            pair_v[...] = (weight * mm(mask, gathered(cot_ref, qy))).astype(BF16)
            c_pair().start()

        return carry

    lax.fori_loop(1, 3, build, 0)
    mask, weight = select(me)
    for part in range(tp):
        routed_v[part, rows(me), :] = (weight * mm(mask, gathered(cot_ref, part))).astype(BF16)

    for load in loads:
        load.wait()

    chunk = min(slots, 256)

    def ahead(some):
        pre_g[some, :] = mm(x_v[some, :], wg_v[...])
        pre_u[some, :] = mm(x_v[some, :], wu_v[...])

    def forward(i, carry):
        ahead(pl.ds(pl.multiple_of(i * chunk, chunk), chunk))
        return carry

    def stage_experts(j):
        block = rows(source(j))
        total = mm(routed_v[0, block, :], gathered(wd_v, 0), NT)
        for part in range(1, tp):
            total = total + mm(routed_v[part, block, :], gathered(wd_v, part), NT)
        gate = pre_g[block, :]
        up = pre_u[block, :]
        sig = jax.nn.sigmoid(gate)
        swish = gate * sig
        hid_v[block, :] = (swish * up).astype(BF16)
        g_gate = (total * up * sig * (1.0 + gate * (1.0 - sig))).astype(BF16)
        g_up = (total * swish).astype(BF16)
        gpg_v[block, :] = g_gate
        gpu_v[block, :] = g_up
        for u in range(2 * tp):
            some = slice(u * du, (u + 1) * du)
            part_v[u % tp, block, u // tp * du : (u // tp + 1) * du] = (
                mm(g_gate, wg_v[some, :], NT) + mm(g_up, wu_v[some, :], NT)
            ).astype(BF16)
        c_core(j, 1).start()
        c_core(j, 0).start()

    def share(j):
        c_out(j).wait_recv()
        c_agd(j).start()

        @pl.when(j != twin)
        def _():
            c_agy(j).start()

    def pass_on(j):
        @pl.when(j != twin)
        def _():
            c_agy(j).wait_recv()

        @pl.when(j == twin)
        def _():
            c_pair().wait_recv()

        c_fwd(j).start()

    def stage_cores(j):
        block = rows(source(j))
        c_core(j, 1).wait_recv()
        ysend_v[block, :] = (
            part_v[qy, block, :].astype(F32) + core_v[1, block, :].astype(F32)
        ).astype(BF16)
        c_y(j).start()

    def stage_return(j):
        block = rows(source(j))
        c_core(j, 0).wait_recv()
        c_y(j).wait_recv()
        total = (
            part_v[q, block, :].astype(F32)
            + core_v[0, block, :].astype(F32)
            + yrecv_v[block, :].astype(F32)
        ).astype(BF16)

        @pl.when(j == 0)
        def _():
            ret_v[block, :] = total

        @pl.when(j > 0)
        def _():
            back_v[block, :] = total
            c_ret(j).start()

    def experts(j):
        c_agd(j).wait_recv()
        c_fwd(j).wait_recv()
        stage_experts(j)

    def pipeline(t, carry):
        @pl.when(t < n - 1)
        def _():
            share(t + 1)

        @pl.when(t < n - 4)
        def _():
            build(t + 4, 0)

        experts(t)

        stage_return(t - 1)

        stage_cores(t)

        @pl.when(t < n - 1)
        def _():
            pass_on(t + 1)

        return carry

    ahead(rows(me))
    stage_experts(0)
    build(3, 0)
    lax.fori_loop(0, slots // chunk // 2, forward, 0)
    stage_cores(0)
    share(1)
    build(4, 0)
    lax.fori_loop(slots // chunk // 2, slots // chunk, forward, 0)
    pass_on(1)
    lax.fori_loop(1, n, pipeline, 0)

    for part in range(tp):
        both = mm(hid_v[...], routed_v[part], TN).astype(BF16)
        gd_v[:, part * du : (part + 1) * du] = both[:, :du]
        gd_v[:, (part + tp) * du : (part + tp + 1) * du] = both[:, du:]
    save_gd = pltpu.make_async_copy(gd_v, gd_hbm.at[0], save_sem.at[1])
    save_gd.start()
    piece = min(width, 512)

    def weights(i, carry):
        some = pl.ds(pl.multiple_of(i * piece, piece), piece)
        flipped = x_v[:, some]
        gg_v[some, :] = mm(flipped, gpg_v[...], TN).astype(BF16)
        gu_v[some, :] = mm(flipped, gpu_v[...], TN).astype(BF16)
        return carry

    lax.fori_loop(0, width // piece // 2, weights, 0)
    stage_return(n - 1)
    lax.fori_loop(width // piece // 2, width // piece, weights, 0)
    save_gg = pltpu.make_async_copy(gg_v, gg_hbm.at[0], save_sem.at[2])
    save_gg.start()
    save_gu = pltpu.make_async_copy(gu_v, gu_hbm.at[0], save_sem.at[3])
    save_gu.start()

    def wait_ret(i, carry):
        c_ret(i).wait_recv()
        return carry

    lax.fori_loop(1, n, wait_ret, 0)
    mine = (gathered(cot_ref, q).astype(F32) + mm(sel_v[...], ret_v[...], TN)).astype(BF16)
    mid_v[q] = mine

    def half_of(part, h):
        return mid_v.at[part, :, h * du : (h + 1) * du]

    mid_y = [remote(half_of(q, h), half_of(q, h), mid_s.at[h], mid_r.at[h], me, qy) for h in (0, 1)]
    mid_f = [
        remote(half_of(qy, h), half_of(qy, h), mid_s.at[h + 2], mid_r.at[h + 2], me, qd)
        for h in (0, 1)
    ]
    mid_d = remote(mid_v.at[q], mid_v.at[q], mid_s.at[4], mid_r.at[4], me, qd)
    mid_y[0].start()
    mid_d.start()
    mid_y[1].start()

    gate_in = gin_ref[...].astype(F32)
    conv_sum = csum_ref[...].astype(F32)
    mixed = (gate_in * conv_sum).astype(BF16)
    own_rows = width // n
    owners = n // (2 * tp)

    def owned(block):
        return pl.ds(pl.multiple_of(block * own_rows, own_rows), own_rows)

    def c_term(block, slot):
        return remote(
            term_v.at[owned(block)], terms_v.at[slot], term_s.at[block], term_r.at[slot], block, q
        )

    def send_terms(part, h):
        some = unit(part, h)
        term_v[some, :] = mm(mid_v[part, :, h * du : (h + 1) * du], mixed, TN).astype(BF16)

        def send(i, carry):
            block = (part + h * tp) * owners + i

            @pl.when(block != me)
            def _():
                c_term(block, me).start()

            return carry

        lax.fori_loop(0, owners, send, 0)

    send_terms(q, 0)
    send_terms(q, 1)
    mid_d.wait_recv()
    send_terms(qd, 0)
    send_terms(qd, 1)
    mid_y[0].wait_recv()
    mid_f[0].start()
    send_terms(qy, 0)
    mid_f[0].wait_recv()
    send_terms(qdy, 0)
    mid_y[1].wait_recv()
    mid_f[1].start()
    send_terms(qy, 1)
    mid_f[1].wait_recv()
    save_gi = [
        pltpu.make_async_copy(
            mid_v.at[
                (2 * q + i) % tp,
                :,
                pl.ds(pl.multiple_of((2 * q + i) // tp * du, du), du),
            ],
            gi_hbm.at[:, i * du : (i + 1) * du],
            save_sem.at[4 * i],
        )
        for i in range(2)
    ]
    for save in save_gi:
        save.start()
    grad_mixed = jnp.zeros((tokens, mixed.shape[1]), F32)
    for u in range(2 * tp):
        grad_mixed = grad_mixed + mm(
            mid_v[u % tp, :, u // tp * du : (u // tp + 1) * du], ow_ref[u * du : (u + 1) * du, :]
        )
    ext_v[:tokens, :] = grad_mixed * gate_in
    edge = halo_v.shape[0]
    halo = remote(ext_v.at[pl.ds(0, edge)], halo_v, halo_s, halo_r, (me - 1 + n) % n, q)
    halo.start()
    send_terms(qdy, 1)
    ggi_out[...] = (grad_mixed * conv_sum).astype(BF16)

    halo.wait_recv()
    ext_v[tokens:, :] = jnp.where(me == n - 1, 0.0, halo_v[...])
    taps = taps_ref[...]
    grad_prod = (
        taps[0:1, :] * ext_v[2 : tokens + 2, :]
        + taps[1:2, :] * ext_v[1 : tokens + 1, :]
        + taps[2:3, :] * ext_v[:tokens, :]
    )
    gcc_out[...] = (grad_prod * cv_ref[...].astype(F32)).astype(BF16)
    gcv_out[...] = (grad_prod * cc_ref[...].astype(F32)).astype(BF16)

    def add_term(i, total):
        other = (me + i) % n
        c_term(other, other).wait_recv()
        return total + terms_v[other].astype(F32)

    gow_out[...] = lax.fori_loop(1, n, add_term, term_v[owned(me), :].astype(F32))

    def drain(i, carry):
        c_out(i).wait_send()
        c_agd(i).wait_send()

        @pl.when(i != twin)
        def _():
            c_agy(i).wait_send()

        c_fwd(i).wait_send()
        c_ret(i).wait_send()
        c_term((me + i) % n, me).wait_send()
        return carry

    lax.fori_loop(1, n, drain, 0)
    c_pair().wait_send()

    def drain_all(i, carry):
        c_core(i, 0).wait_send()
        c_core(i, 1).wait_send()
        c_y(i).wait_send()
        return carry

    lax.fori_loop(0, n, drain_all, 0)
    mid_d.wait_send()
    for h in (0, 1):
        mid_y[h].wait_send()
        mid_f[h].wait_send()
    halo.wait_send()
    for save in (*save_gi, save_gd, save_gg, save_gu):
        save.wait()


def move(*refs):
    count = (len(refs) - 2) // 3
    sources, targets, held = refs[:count], refs[count : 2 * count], refs[2 * count : 3 * count]
    in_sem, out_sem = refs[-2:]
    ins = [pltpu.make_async_copy(sources[i], held[i], in_sem.at[i]) for i in range(count)]
    outs = [pltpu.make_async_copy(held[i], targets[i], out_sem.at[i]) for i in range(count)]
    for copy in ins:
        copy.start()
    for i in range(count):
        ins[i].wait()
        outs[i].start()
    for copy in outs:
        copy.wait()


def moved(arrays):
    count = len(arrays)
    hbm = pl.BlockSpec(memory_space=pl.ANY)
    return pl.pallas_call(
        move,
        out_shape=tuple(jax.ShapeDtypeStruct(a.shape, a.dtype) for a in arrays),
        in_specs=[hbm] * count,
        out_specs=(hbm,) * count,
        scratch_shapes=[pltpu.VMEM(a.shape, a.dtype) for a in arrays]
        + [pltpu.SemaphoreType.DMA((count,))] * 2,
        compiler_params=pltpu.CompilerParams(vmem_limit_bytes=60 * 1024 * 1024),
    )(*arrays)


def body(
    cotangent,
    route_ids,
    route_weights,
    expert_inputs,
    gate_weight,
    up_weight,
    down_weight,
    out_weight,
    gate_in,
    conv_sum,
    conv_c,
    conv_v,
    conv_taps,
):
    n = lax.axis_size("sp")
    tp = lax.axis_size("tp")
    tokens, width = cotangent.shape
    slots = expert_inputs.shape[1]
    hidden = gate_weight.shape[2]
    chans = gate_in.shape[1]
    dq = width // tp
    vmem = pl.BlockSpec(memory_space=pltpu.VMEM)
    hbm = pl.BlockSpec(memory_space=pl.ANY)
    dma = pltpu.SemaphoreType.DMA
    results = pl.pallas_call(
        functools.partial(kernel, n, tp),
        out_shape=(
            jax.ShapeDtypeStruct((tokens, dq), BF16),
            jax.ShapeDtypeStruct(gate_weight.shape, BF16),
            jax.ShapeDtypeStruct(up_weight.shape, BF16),
            jax.ShapeDtypeStruct(down_weight.shape, BF16),
            jax.ShapeDtypeStruct((width // n, chans), F32),
            jax.ShapeDtypeStruct((tokens, chans), BF16),
            jax.ShapeDtypeStruct((tokens, chans), BF16),
            jax.ShapeDtypeStruct((tokens, chans), BF16),
        ),
        in_specs=[vmem] * 3 + [hbm] * 4 + [vmem] * 6,
        out_specs=(hbm,) * 4 + (vmem,) * 4,
        scratch_shapes=[
            pltpu.VMEM((slots, width), BF16),
            pltpu.VMEM((width, hidden), BF16),
            pltpu.VMEM((width, hidden), BF16),
            pltpu.VMEM((hidden, width), BF16),
            pltpu.VMEM((slots, tokens), BF16),
            pltpu.VMEM((slots, dq), BF16),
            pltpu.VMEM((slots // n, dq), BF16),
            pltpu.VMEM((tp, slots, dq), BF16),
            pltpu.VMEM((slots, hidden), F32),
            pltpu.VMEM((slots, hidden), F32),
            pltpu.VMEM((slots, hidden), BF16),
            pltpu.VMEM((slots, hidden), BF16),
            pltpu.VMEM((slots, hidden), BF16),
            pltpu.VMEM((tp, slots, dq), BF16),
            pltpu.VMEM((2, slots, dq), BF16),
            pltpu.VMEM((slots, dq), BF16),
            pltpu.VMEM((slots, dq), BF16),
            pltpu.VMEM((slots, dq), BF16),
            pltpu.VMEM((slots, dq), BF16),
            pltpu.VMEM((tp, tokens, dq), BF16),
            pltpu.VMEM((width, chans), BF16),
            pltpu.VMEM((n, width // n, chans), BF16),
            pltpu.VMEM((tokens + 8, chans), F32),
            pltpu.VMEM((8, chans), F32),
            pltpu.VMEM((width, hidden), BF16),
            pltpu.VMEM((width, hidden), BF16),
            pltpu.VMEM((hidden, width), BF16),
            dma((4,)),
            dma((5,)),
            dma((n,)),
            dma((n,)),
            dma(()),
            dma(()),
            dma((n,)),
            dma((n,)),
            dma((n,)),
            dma((n,)),
            dma((n,)),
            dma((n,)),
            dma((2, n)),
            dma((2, n)),
            dma((n,)),
            dma((n,)),
            dma((n,)),
            dma((n,)),
            dma((5,)),
            dma((5,)),
            dma((n,)),
            dma((n,)),
            dma(()),
            dma(()),
        ],
        compiler_params=pltpu.CompilerParams(
            collective_id=0, has_side_effects=True, vmem_limit_bytes=60 * 1024 * 1024
        ),
    )(
        route_ids.T,
        route_weights.T,
        cotangent,
        expert_inputs,
        gate_weight,
        up_weight,
        down_weight,
        out_weight,
        gate_in,
        conv_sum,
        conv_c,
        conv_v,
        conv_taps,
    )
    return moved(results)


def solution(mesh):
    placed = (
        P("sp", None),
        P("sp", None),
        P("sp", None),
        P("sp", None, None),
        P("sp", None, "tp"),
        P("sp", None, "tp"),
        P("sp", "tp", None),
        P(None, "tp"),
        P("sp", "tp"),
        P("sp", "tp"),
        P("sp", "tp"),
        P("sp", "tp"),
        P(None, "tp"),
    )
    return jax.shard_map(
        body,
        mesh=mesh,
        in_specs=placed,
        out_specs=(
            P("sp", "tp"),
            P("sp", None, "tp"),
            P("sp", None, "tp"),
            P("sp", "tp", None),
            P("sp", "tp"),
            P("sp", "tp"),
            P("sp", "tp"),
            P("sp", "tp"),
        ),
        check_vma=False,
    )
```

profile of v0, /device:TPU:26, one launch (start us, length us, event | category | flops | bytes accessed | tf_op | source)
XLA Modules:
  0.0 85.5 jit_solution(6967684469480015433)
XLA Ops:
  0.6 81.7 %shard_map.188 = (bf16[256,512]{1,0:T(8,128)(2,1)}, bf16[1,2048,256]{2,1,0:T(8,128)(2,1)}, bf16[1,2048,256]{2,1,0:T(8,128)(2,1)}, bf16[1,256,2048]{2,1,0:T(8,128...) custom-call(s32[2,256]{1,0:T(2,128)} %bitcast.2, ...), custom_call_target="tpu_custom_call" | custom-call | tf_op jit(solution)/shard_map/pallas_call | solution.py:596
  82.3 3.2 %shard_map.189 = (bf16[256,512]{1,0:T(8,128)(2,1)}, bf16[1,2048,256]{2,1,0:T(8,128)(2,1)}, bf16[1,2048,256]{2,1,0:T(8,128)(2,1)}, bf16[1,256,2048]{2,1,0:T(8,128...) custom-call(bf16[256,512]{1,0:T(8,128)(2,1)} %get-tuple-element.16.r, ...), custom_call_target="tpu_custom_call" | custom-call | tf_op jit(solution)/shard_map/pallas_call | solution.py:560
where the time goes:
time: 86.1 us; the launch traced here: 85.5 us
  Pallas kernels  84.9 us (99%)
    pallas_call x1, Pallas kernels, body(): pl.pallas_call(functools.partial(kernel, n, tp), out_shape=(jax.ShapeDtyp...  81.7 us
    pallas_call x1, Pallas kernels, moved(): pl.pallas_call(move, out_shape=tuple((jax.ShapeDtypeStruct(a.shape, a.dty...  3.24 us

commit v1 on v0

--- a/solution.py
+++ b/solution.py
@@ -20,27 +20,36 @@
 def kernel(
     n,
     tp,
-    ids_ref,
-    wts_ref,
-    cot_ref,
+    ids_hbm,
+    wts_hbm,
+    cot_hbm,
     x_hbm,
     wg_hbm,
     wu_hbm,
     wd_hbm,
+    ow_hbm,
+    gin_hbm,
+    csum_hbm,
+    cc_hbm,
+    cv_hbm,
+    taps_hbm,
+    gi_out,
+    gg_out,
+    gu_out,
+    gd_out,
+    gow_out,
+    ggi_out,
+    gcc_out,
+    gcv_out,
+    ids_ref,
+    wts_ref,
+    cot_ref,
     ow_ref,
     gin_ref,
     csum_ref,
     cc_ref,
     cv_ref,
     taps_ref,
-    gi_hbm,
-    gg_hbm,
-    gu_hbm,
-    gd_hbm,
-    gow_out,
-    ggi_out,
-    gcc_out,
-    gcv_out,
     x_v,
     wg_v,
     wu_v,
@@ -65,11 +74,8 @@
     terms_v,
     ext_v,
     halo_v,
-    gg_v,
-    gu_v,
-    gd_v,
     load_sem,
-    save_sem,
+    side_sem,
     out_s,
     out_r,
     pair_s,
@@ -105,15 +111,6 @@
     du = dq // 2
     top = ids_ref.shape[0]
 
-    loads = [
-        pltpu.make_async_copy(src.at[0], dst, load_sem.at[i])
-        for i, (src, dst) in enumerate(
-            ((x_hbm, x_v), (wg_hbm, wg_v), (wu_hbm, wu_v), (wd_hbm, wd_v))
-        )
-    ]
-    for load in loads:
-        load.start()
-
     barrier = pltpu.get_barrier_semaphore()
 
     def greet(i, carry):
@@ -127,6 +124,35 @@
         pl.semaphore_signal(
             barrier, inc=1, device_id=(me, other), device_id_type=pl.DeviceIdType.MESH
         )
+
+    first_loads = [
+        pltpu.make_async_copy(src, dst, side_sem.at[i])
+        for i, (src, dst) in enumerate(
+            ((ids_hbm, ids_ref), (wts_hbm, wts_ref), (cot_hbm, cot_ref))
+        )
+    ]
+    loads = [
+        pltpu.make_async_copy(src.at[0], dst, load_sem.at[i])
+        for i, (src, dst) in enumerate(
+            ((wg_hbm, wg_v), (wu_hbm, wu_v), (wd_hbm, wd_v), (x_hbm, x_v))
+        )
+    ]
+    late_loads = [
+        pltpu.make_async_copy(src, dst, side_sem.at[i + 3])
+        for i, (src, dst) in enumerate(
+            (
+                (ow_hbm, ow_ref),
+                (gin_hbm, gin_ref),
+                (csum_hbm, csum_ref),
+                (cc_hbm, cc_ref),
+                (cv_hbm, cv_ref),
+                (taps_hbm, taps_ref),
+            )
+        )
+    ]
+
+    for load in (*first_loads, *loads, *late_loads):
+        load.start()
 
     def rows(block):
         return pl.ds(pl.multiple_of(block * cap, cap), cap)
@@ -152,13 +178,18 @@
     side, low = me // half, me % half
     pair, member = low // 2, low % 2
 
-    twin = n - 1
+    def index(p):
+        far = jnp.where(p == 2, half, half + p - 3)
+        near = jnp.where(p < 2, p, jnp.where(p == 3, 2, p - half))
+        return jnp.where((p == 2) | ((p > 3) & (p < half + 3)), far, near)
+
+    def across_at(p):
+        return index(p) >= half
 
     def step(p):
-        far = (p == 1) | ((p >= 3) & (p < half + 2))
-        across = jnp.where(far, 1, 0)
-        late = jnp.where(p < 3, p, jnp.where(p == twin, 1, p - half + 1))
-        turn = jnp.where(far, jnp.where(p == 1, 0, p - 2), late)
+        i = index(p)
+        across = jnp.where(i >= half, 1, 0)
+        turn = i % half
         return (side + across) % 2 * half, turn // 2, turn % 2
 
     def to(i):
@@ -174,8 +205,15 @@
             sent_v.at[rows(to(i))], routed_v.at[q, rows(me)], out_s.at[i], out_r.at[i], to(i), q
         )
 
-    def c_pair():
-        return remote(pair_v, routed_v.at[qy, rows(me)], pair_s, pair_r, to(twin), q)
+    def c_pair(i):
+        return remote(
+            pair_v.at[rows(to(i))],
+            routed_v.at[qy, rows(me)],
+            pair_s.at[i],
+            pair_r.at[i],
+            to(i),
+            q,
+        )
 
     def c_agy(i):
         block = routed_v.at[q, rows(source(i))]
@@ -208,6 +246,8 @@
             back_v.at[rows(source(i))], ret_v.at[rows(me)], ret_s.at[i], ret_r.at[i], source(i), q
         )
 
+    for load in first_loads:
+        load.wait()
     ids = ids_ref[...]
     experts = n
     e_iota = lax.broadcasted_iota(jnp.int32, (experts, tokens), 0)
@@ -246,14 +286,14 @@
         sent_v[rows(to(i)), :] = (weight * mm(mask, gathered(cot_ref, q))).astype(BF16)
         c_out(i).start()
 
-        @pl.when(i == twin)
-        def _():
-            pair_v[...] = (weight * mm(mask, gathered(cot_ref, qy))).astype(BF16)
-            c_pair().start()
+        @pl.when(jnp.logical_not(across_at(i)))
+        def _():
+            pair_v[rows(to(i)), :] = (weight * mm(mask, gathered(cot_ref, qy))).astype(BF16)
+            c_pair(i).start()
 
         return carry
 
-    lax.fori_loop(1, 3, build, 0)
+    lax.fori_loop(1, 4, build, 0)
     mask, weight = select(me)
     for part in range(tp):
         routed_v[part, rows(me), :] = (weight * mm(mask, gathered(cot_ref, part))).astype(BF16)
@@ -297,18 +337,18 @@
         c_out(j).wait_recv()
         c_agd(j).start()
 
-        @pl.when(j != twin)
+        @pl.when(across_at(j))
         def _():
             c_agy(j).start()
 
     def pass_on(j):
-        @pl.when(j != twin)
+        @pl.when(across_at(j))
         def _():
             c_agy(j).wait_recv()
 
-        @pl.when(j == twin)
-        def _():
-            c_pair().wait_recv()
+        @pl.when(jnp.logical_not(across_at(j)))
+        def _():
+            c_pair(j).wait_recv()
 
         c_fwd(j).start()
 
@@ -345,7 +385,7 @@
         stage_experts(j)
 
     def pipeline(t, carry):
-        @pl.when(t < n - 1)
+        @pl.when(t < 4)
         def _():
             share(t + 1)
 
@@ -355,9 +395,13 @@
 
         experts(t)
 
+        stage_cores(t)
+
         stage_return(t - 1)
 
-        stage_cores(t)
+        @pl.when(jnp.logical_and(t + 1 >= 4, t < n - 2))
+        def _():
+            share(t + 2)
 
         @pl.when(t < n - 1)
         def _():
@@ -367,37 +411,30 @@
 
     ahead(rows(me))
     stage_experts(0)
-    build(3, 0)
+    build(4, 0)
     lax.fori_loop(0, slots // chunk // 2, forward, 0)
     stage_cores(0)
     share(1)
-    build(4, 0)
     lax.fori_loop(slots // chunk // 2, slots // chunk, forward, 0)
     pass_on(1)
     lax.fori_loop(1, n, pipeline, 0)
 
     for part in range(tp):
         both = mm(hid_v[...], routed_v[part], TN).astype(BF16)
-        gd_v[:, part * du : (part + 1) * du] = both[:, :du]
-        gd_v[:, (part + tp) * du : (part + tp + 1) * du] = both[:, du:]
-    save_gd = pltpu.make_async_copy(gd_v, gd_hbm.at[0], save_sem.at[1])
-    save_gd.start()
+        gd_out[0, :, part * du : (part + 1) * du] = both[:, :du]
+        gd_out[0, :, (part + tp) * du : (part + tp + 1) * du] = both[:, du:]
     piece = min(width, 512)
 
     def weights(i, carry):
         some = pl.ds(pl.multiple_of(i * piece, piece), piece)
         flipped = x_v[:, some]
-        gg_v[some, :] = mm(flipped, gpg_v[...], TN).astype(BF16)
-        gu_v[some, :] = mm(flipped, gpu_v[...], TN).astype(BF16)
+        gg_out[0, some, :] = mm(flipped, gpg_v[...], TN).astype(BF16)
+        gu_out[0, some, :] = mm(flipped, gpu_v[...], TN).astype(BF16)
         return carry
 
     lax.fori_loop(0, width // piece // 2, weights, 0)
     stage_return(n - 1)
     lax.fori_loop(width // piece // 2, width // piece, weights, 0)
-    save_gg = pltpu.make_async_copy(gg_v, gg_hbm.at[0], save_sem.at[2])
-    save_gg.start()
-    save_gu = pltpu.make_async_copy(gu_v, gu_hbm.at[0], save_sem.at[3])
-    save_gu.start()
 
     def wait_ret(i, carry):
         c_ret(i).wait_recv()
@@ -420,6 +457,8 @@
     mid_d.start()
     mid_y[1].start()
 
+    for load in late_loads:
+        load.wait()
     gate_in = gin_ref[...].astype(F32)
     conv_sum = csum_ref[...].astype(F32)
     mixed = (gate_in * conv_sum).astype(BF16)
@@ -463,20 +502,6 @@
     mid_f[1].start()
     send_terms(qy, 1)
     mid_f[1].wait_recv()
-    save_gi = [
-        pltpu.make_async_copy(
-            mid_v.at[
-                (2 * q + i) % tp,
-                :,
-                pl.ds(pl.multiple_of((2 * q + i) // tp * du, du), du),
-            ],
-            gi_hbm.at[:, i * du : (i + 1) * du],
-            save_sem.at[4 * i],
-        )
-        for i in range(2)
-    ]
-    for save in save_gi:
-        save.start()
     grad_mixed = jnp.zeros((tokens, mixed.shape[1]), F32)
     for u in range(2 * tp):
         grad_mixed = grad_mixed + mm(
@@ -487,6 +512,11 @@
     halo = remote(ext_v.at[pl.ds(0, edge)], halo_v, halo_s, halo_r, (me - 1 + n) % n, q)
     halo.start()
     send_terms(qdy, 1)
+    for i in range(2):
+        own = 2 * q + i
+        gi_out[:, i * du : (i + 1) * du] = mid_v[
+            own % tp, :, pl.ds(pl.multiple_of(own // tp * du, du), du)
+        ]
     ggi_out[...] = (grad_mixed * conv_sum).astype(BF16)
 
     halo.wait_recv()
@@ -511,9 +541,13 @@
         c_out(i).wait_send()
         c_agd(i).wait_send()
 
-        @pl.when(i != twin)
+        @pl.when(across_at(i))
         def _():
             c_agy(i).wait_send()
+
+        @pl.when(jnp.logical_not(across_at(i)))
+        def _():
+            c_pair(i).wait_send()
 
         c_fwd(i).wait_send()
         c_ret(i).wait_send()
@@ -521,7 +555,6 @@
         return carry
 
     lax.fori_loop(1, n, drain, 0)
-    c_pair().wait_send()
 
     def drain_all(i, carry):
         c_core(i, 0).wait_send()
@@ -535,36 +568,28 @@
         mid_y[h].wait_send()
         mid_f[h].wait_send()
     halo.wait_send()
-    for save in (*save_gi, save_gd, save_gg, save_gu):
-        save.wait()
 
 
 def move(*refs):
-    count = (len(refs) - 2) // 3
-    sources, targets, held = refs[:count], refs[count : 2 * count], refs[2 * count : 3 * count]
-    in_sem, out_sem = refs[-2:]
-    ins = [pltpu.make_async_copy(sources[i], held[i], in_sem.at[i]) for i in range(count)]
-    outs = [pltpu.make_async_copy(held[i], targets[i], out_sem.at[i]) for i in range(count)]
-    for copy in ins:
+    count = (len(refs) - 1) // 2
+    outs = [
+        pltpu.make_async_copy(refs[i], refs[count + i], refs[-1].at[i]) for i in range(count)
+    ]
+    for copy in outs:
         copy.start()
-    for i in range(count):
-        ins[i].wait()
-        outs[i].start()
     for copy in outs:
         copy.wait()
 
 
 def moved(arrays):
     count = len(arrays)
-    hbm = pl.BlockSpec(memory_space=pl.ANY)
     return pl.pallas_call(
         move,
         out_shape=tuple(jax.ShapeDtypeStruct(a.shape, a.dtype) for a in arrays),
-        in_specs=[hbm] * count,
-        out_specs=(hbm,) * count,
-        scratch_shapes=[pltpu.VMEM(a.shape, a.dtype) for a in arrays]
-        + [pltpu.SemaphoreType.DMA((count,))] * 2,
-        compiler_params=pltpu.CompilerParams(vmem_limit_bytes=60 * 1024 * 1024),
+        in_specs=[pl.BlockSpec(memory_space=pltpu.VMEM)] * count,
+        out_specs=(pl.BlockSpec(memory_space=pl.ANY),) * count,
+        scratch_shapes=[pltpu.SemaphoreType.DMA((count,))],
+        compiler_params=pltpu.CompilerParams(vmem_limit_bytes=16000 * 1024),
     )(*arrays)
 
 
@@ -589,6 +614,7 @@
     slots = expert_inputs.shape[1]
     hidden = gate_weight.shape[2]
     chans = gate_in.shape[1]
+    top = route_ids.shape[1]
     dq = width // tp
     vmem = pl.BlockSpec(memory_space=pltpu.VMEM)
     hbm = pl.BlockSpec(memory_space=pl.ANY)
@@ -596,25 +622,34 @@
     results = pl.pallas_call(
         functools.partial(kernel, n, tp),
         out_shape=(
-            jax.ShapeDtypeStruct((tokens, dq), BF16),
-            jax.ShapeDtypeStruct(gate_weight.shape, BF16),
-            jax.ShapeDtypeStruct(up_weight.shape, BF16),
-            jax.ShapeDtypeStruct(down_weight.shape, BF16),
-            jax.ShapeDtypeStruct((width // n, chans), F32),
-            jax.ShapeDtypeStruct((tokens, chans), BF16),
-            jax.ShapeDtypeStruct((tokens, chans), BF16),
-            jax.ShapeDtypeStruct((tokens, chans), BF16),
+            pltpu.VMEM((tokens, dq), BF16),
+            pltpu.VMEM(gate_weight.shape, BF16),
+            pltpu.VMEM(up_weight.shape, BF16),
+            pltpu.VMEM(down_weight.shape, BF16),
+            pltpu.VMEM((width // n, chans), F32),
+            pltpu.VMEM((tokens, chans), BF16),
+            pltpu.VMEM((tokens, chans), BF16),
+            pltpu.VMEM((tokens, chans), BF16),
         ),
-        in_specs=[vmem] * 3 + [hbm] * 4 + [vmem] * 6,
-        out_specs=(hbm,) * 4 + (vmem,) * 4,
+        in_specs=[hbm] * 13,
+        out_specs=(vmem,) * 8,
         scratch_shapes=[
+            pltpu.VMEM((top, tokens), jnp.int32),
+            pltpu.VMEM((top, tokens), F32),
+            pltpu.VMEM((tokens, width), BF16),
+            pltpu.VMEM((width, chans), BF16),
+            pltpu.VMEM((tokens, chans), BF16),
+            pltpu.VMEM((tokens, chans), BF16),
+            pltpu.VMEM((tokens, chans), BF16),
+            pltpu.VMEM((tokens, chans), BF16),
+            pltpu.VMEM(conv_taps.shape, F32),
             pltpu.VMEM((slots, width), BF16),
             pltpu.VMEM((width, hidden), BF16),
             pltpu.VMEM((width, hidden), BF16),
             pltpu.VMEM((hidden, width), BF16),
             pltpu.VMEM((slots, tokens), BF16),
             pltpu.VMEM((slots, dq), BF16),
-            pltpu.VMEM((slots // n, dq), BF16),
+            pltpu.VMEM((slots, dq), BF16),
             pltpu.VMEM((tp, slots, dq), BF16),
             pltpu.VMEM((slots, hidden), F32),
             pltpu.VMEM((slots, hidden), F32),
@@ -632,15 +667,12 @@
             pltpu.VMEM((n, width // n, chans), BF16),
             pltpu.VMEM((tokens + 8, chans), F32),
             pltpu.VMEM((8, chans), F32),
-            pltpu.VMEM((width, hidden), BF16),
-            pltpu.VMEM((width, hidden), BF16),
-            pltpu.VMEM((hidden, width), BF16),
             dma((4,)),
-            dma((5,)),
-            dma((n,)),
-            dma((n,)),
-            dma(()),
-            dma(()),
+            dma((9,)),
+            dma((n,)),
+            dma((n,)),
+            dma((n,)),
+            dma((n,)),
             dma((n,)),
             dma((n,)),
             dma((n,)),
@@ -661,7 +693,7 @@
             dma(()),
         ],
         compiler_params=pltpu.CompilerParams(
-            collective_id=0, has_side_effects=True, vmem_limit_bytes=60 * 1024 * 1024
+            collective_id=0, has_side_effects=True, vmem_limit_bytes=61696 * 1024
         ),
     )(
         route_ids.T,

time: 86.1 us -> 79.1 us (0.919)
  Pallas kernels: 84.9 us -> 78.1 us
    pallas_call x1, Pallas kernels: 81.7 us -> 76.2 us  [body(): pl.pallas_call(functools.partial(kernel, n, tp), out_shape=(pltpu.VMEM((t...]
    pallas_call x1, Pallas kernels: 3.24 us -> 1.91 us  [moved(): pl.pallas_call(move, out_shape=tuple((jax.ShapeDtypeStruct(a.shape, a.dty...]
where the time goes in v1:
time: 79.1 us; the launch traced here: 78.8 us
  Pallas kernels  78.1 us (99%)
    pallas_call x1, Pallas kernels, body(): pl.pallas_call(functools.partial(kernel, n, tp), out_shape=(pltpu.VMEM((t...  76.2 us
    pallas_call x1, Pallas kernels, moved(): pl.pallas_call(move, out_shape=tuple((jax.ShapeDtypeStruct(a.shape, a.dty...  1.91 us

profile of v1, /device:TPU:26, one launch (start us, length us, event | category | flops | bytes accessed | tf_op | source)
XLA Modules:
  0.0 78.8 jit_solution(16309424081613230875)
XLA Ops:
  0.6 76.2 %shard_map.188 = (bf16[256,512]{1,0:T(8,128)(2,1)S(1)}, bf16[1,2048,256]{2,1,0:T(8,128)(2,1)S(1)}, bf16[1,2048,256]{2,1,0:T(8,128)(2,1)S(1)}, bf16[1,256,2048]{2...) custom-call(s32[2,256]{1,0:T(2,128)} %bitcast.2, ...), custom_call_target="tpu_custom_call" | custom-call | tf_op jit(solution)/shard_map/pallas_call | solution.py:622
  76.8 1.9 %shard_map.189 = (bf16[256,512]{1,0:T(8,128)(2,1)}, bf16[1,2048,256]{2,1,0:T(8,128)(2,1)}, bf16[1,2048,256]{2,1,0:T(8,128)(2,1)}, bf16[1,256,2048]{2,1,0:T(8,128...) custom-call(bf16[256,512]{1,0:T(8,128)(2,1)S(1)} %get-tuple-element., ...), custom_call_target="tpu_custom_call" | custom-call | tf_op jit(solution)/shard_map/pallas_call | solution.py:586

commit v2 on v1

--- a/solution.py
+++ b/solution.py
@@ -77,26 +77,24 @@
     load_sem,
     side_sem,
     out_s,
+    pair_s,
+    agy_s,
+    agd_s,
+    fwd_s,
+    core_s,
+    y_s,
+    ret_s,
+    term_s,
+    mid_s,
+    halo_s,
     out_r,
-    pair_s,
-    pair_r,
-    agy_s,
     agy_r,
-    agd_s,
-    agd_r,
-    fwd_s,
-    fwd_r,
-    core_s,
+    core_in,
     core_r,
-    y_s,
     y_r,
-    ret_s,
     ret_r,
-    mid_s,
+    term_r,
     mid_r,
-    term_s,
-    term_r,
-    halo_s,
     halo_r,
 ):
     me = lax.axis_index("sp")
@@ -179,7 +177,8 @@
     pair, member = low // 2, low % 2
 
     def index(p):
-        far = jnp.where(p == 2, half, half + p - 3)
+        swapped = jnp.where((p == half + 1) | (p == half + 2), 2 * half - p, p - 3)
+        far = half + jnp.where(p == 2, 0, swapped)
         near = jnp.where(p < 2, p, jnp.where(p == 3, 2, p - half))
         return jnp.where((p == 2) | ((p > 3) & (p < half + 3)), far, near)
 
@@ -202,36 +201,36 @@
 
     def c_out(i):
         return remote(
-            sent_v.at[rows(to(i))], routed_v.at[q, rows(me)], out_s.at[i], out_r.at[i], to(i), q
+            sent_v.at[rows(to(i))], routed_v.at[q, rows(me)], out_s, out_r.at[i], to(i), q
         )
 
     def c_pair(i):
         return remote(
             pair_v.at[rows(to(i))],
             routed_v.at[qy, rows(me)],
-            pair_s.at[i],
-            pair_r.at[i],
+            pair_s,
+            agy_r.at[i],
             to(i),
             q,
         )
 
     def c_agy(i):
         block = routed_v.at[q, rows(source(i))]
-        return remote(block, block, agy_s.at[i], agy_r.at[i], me, qy)
+        return remote(block, block, agy_s, agy_r.at[i], me, qy)
 
     def c_agd(i):
         block = routed_v.at[q, rows(source(i))]
-        return remote(block, block, agd_s.at[i], agd_r.at[i], me, qd)
+        return remote(block, block, agd_s, core_in.at[i], me, qd)
 
     def c_fwd(i):
         block = routed_v.at[qy, rows(source(i))]
-        return remote(block, block, fwd_s.at[i], fwd_r.at[i], me, qd)
+        return remote(block, block, fwd_s, core_in.at[i], me, qd)
 
     def c_core(i, h):
         return remote(
             part_v.at[(qd, qdy)[h], rows(source(i))],
             core_v.at[h, rows(source(i))],
-            core_s.at[h, i],
+            core_s,
             core_r.at[h, i],
             me,
             qd,
@@ -239,11 +238,11 @@
 
     def c_y(i):
         block = rows(source(i))
-        return remote(ysend_v.at[block], yrecv_v.at[block], y_s.at[i], y_r.at[i], me, qy)
+        return remote(ysend_v.at[block], yrecv_v.at[block], y_s, y_r.at[i], me, qy)
 
     def c_ret(i):
         return remote(
-            back_v.at[rows(source(i))], ret_v.at[rows(me)], ret_s.at[i], ret_r.at[i], source(i), q
+            back_v.at[rows(source(i))], ret_v.at[rows(me)], ret_s, ret_r, source(i), q
         )
 
     for load in first_loads:
@@ -293,7 +292,9 @@
 
         return carry
 
-    lax.fori_loop(1, 4, build, 0)
+    build(2, 0)
+    build(1, 0)
+    build(3, 0)
     mask, weight = select(me)
     for part in range(tp):
         routed_v[part, rows(me), :] = (weight * mm(mask, gathered(cot_ref, part))).astype(BF16)
@@ -379,9 +380,12 @@
             back_v[block, :] = total
             c_ret(j).start()
 
+    def several(block, count):
+        return block.at[pl.ds(0, count * cap)]
+
     def experts(j):
-        c_agd(j).wait_recv()
-        c_fwd(j).wait_recv()
+        both = several(sent_v, 2)
+        remote(both, both, agd_s, core_in.at[j], me, qd).wait_recv()
         stage_experts(j)
 
     def pipeline(t, carry):
@@ -399,9 +403,13 @@
 
         stage_return(t - 1)
 
-        @pl.when(jnp.logical_and(t + 1 >= 4, t < n - 2))
+        @pl.when(t == 3)
         def _():
             share(t + 2)
+
+        @pl.when(jnp.logical_and(t >= 3, t < n - 3))
+        def _():
+            share(t + 3)
 
         @pl.when(t < n - 1)
         def _():
@@ -436,26 +444,23 @@
     stage_return(n - 1)
     lax.fori_loop(width // piece // 2, width // piece, weights, 0)
 
-    def wait_ret(i, carry):
-        c_ret(i).wait_recv()
-        return carry
-
-    lax.fori_loop(1, n, wait_ret, 0)
-    mine = (gathered(cot_ref, q).astype(F32) + mm(sel_v[...], ret_v[...], TN)).astype(BF16)
-    mid_v[q] = mine
+    back = several(back_v, n - 1)
+    remote(back, back, ret_s, ret_r, me, qd).wait_recv()
 
     def half_of(part, h):
         return mid_v.at[part, :, h * du : (h + 1) * du]
 
-    mid_y = [remote(half_of(q, h), half_of(q, h), mid_s.at[h], mid_r.at[h], me, qy) for h in (0, 1)]
-    mid_f = [
-        remote(half_of(qy, h), half_of(qy, h), mid_s.at[h + 2], mid_r.at[h + 2], me, qd)
-        for h in (0, 1)
-    ]
-    mid_d = remote(mid_v.at[q], mid_v.at[q], mid_s.at[4], mid_r.at[4], me, qd)
-    mid_y[0].start()
-    mid_d.start()
-    mid_y[1].start()
+    def passed(part, h, k, there):
+        return remote(half_of(part, h), half_of(part, h), mid_s, mid_r.at[2 * k + h], me, there)
+
+    mid_y = [passed(q, h, 0, qy) for h in (0, 1)]
+    mid_d = [passed(q, h, 1, qd) for h in (0, 1)]
+    mid_f = [passed(qy, h, 2, qd) for h in (0, 1)]
+    for h in (0, 1):
+        come = mm(sel_v[...], ret_v[:, h * du : (h + 1) * du], TN)
+        mid_v[q, :, h * du : (h + 1) * du] = (cot_ref[:, unit(q, h)].astype(F32) + come).astype(BF16)
+        mid_y[h].start()
+        mid_d[h].start()
 
     for load in late_loads:
         load.wait()
@@ -470,7 +475,7 @@
 
     def c_term(block, slot):
         return remote(
-            term_v.at[owned(block)], terms_v.at[slot], term_s.at[block], term_r.at[slot], block, q
+            term_v.at[owned(block)], terms_v.at[slot], term_s, term_r, block, q
         )
 
     def send_terms(part, h):
@@ -490,9 +495,9 @@
 
     send_terms(q, 0)
     send_terms(q, 1)
-    mid_d.wait_recv()
-    send_terms(qd, 0)
-    send_terms(qd, 1)
+    for h in (0, 1):
+        mid_d[h].wait_recv()
+        send_terms(qd, h)
     mid_y[0].wait_recv()
     mid_f[0].start()
     send_terms(qy, 0)
@@ -530,43 +535,29 @@
     gcc_out[...] = (grad_prod * cv_ref[...].astype(F32)).astype(BF16)
     gcv_out[...] = (grad_prod * cc_ref[...].astype(F32)).astype(BF16)
 
+    parts = terms_v.at[pl.ds(0, n - 1)]
+    remote(parts, parts, term_s, term_r, me, qd).wait_recv()
+
     def add_term(i, total):
-        other = (me + i) % n
-        c_term(other, other).wait_recv()
-        return total + terms_v[other].astype(F32)
+        return total + terms_v[(me + i) % n].astype(F32)
 
     gow_out[...] = lax.fori_loop(1, n, add_term, term_v[owned(me), :].astype(F32))
 
-    def drain(i, carry):
-        c_out(i).wait_send()
-        c_agd(i).wait_send()
-
-        @pl.when(across_at(i))
-        def _():
-            c_agy(i).wait_send()
-
-        @pl.when(jnp.logical_not(across_at(i)))
-        def _():
-            c_pair(i).wait_send()
-
-        c_fwd(i).wait_send()
-        c_ret(i).wait_send()
-        c_term((me + i) % n, me).wait_send()
-        return carry
-
-    lax.fori_loop(1, n, drain, 0)
-
-    def drain_all(i, carry):
-        c_core(i, 0).wait_send()
-        c_core(i, 1).wait_send()
-        c_y(i).wait_send()
-        return carry
-
-    lax.fori_loop(0, n, drain_all, 0)
-    mid_d.wait_send()
-    for h in (0, 1):
-        mid_y[h].wait_send()
-        mid_f[h].wait_send()
+    for sem, block, count in (
+        (out_s, sent_v, n - 1),
+        (pair_s, sent_v, half - 1),
+        (agy_s, sent_v, half),
+        (agd_s, sent_v, n - 1),
+        (fwd_s, sent_v, n - 1),
+        (y_s, sent_v, n),
+        (ret_s, sent_v, n - 1),
+    ):
+        some = several(block, count)
+        remote(some, some, sem, halo_r, me, qd).wait_send()
+    remote(core_v, core_v, core_s, halo_r, me, qd).wait_send()
+    remote(parts, parts, term_s, term_r, me, qd).wait_send()
+    thrice = mid_v.at[pl.ds(0, 3)]
+    remote(thrice, thrice, mid_s, halo_r, me, qd).wait_send()
     halo.wait_send()
 
 
@@ -669,27 +660,17 @@
             pltpu.VMEM((8, chans), F32),
             dma((4,)),
             dma((9,)),
-            dma((n,)),
-            dma((n,)),
-            dma((n,)),
-            dma((n,)),
-            dma((n,)),
-            dma((n,)),
-            dma((n,)),
+        ]
+        + [dma(())] * 11
+        + [
             dma((n,)),
             dma((n,)),
             dma((n,)),
             dma((2, n)),
-            dma((2, n)),
-            dma((n,)),
-            dma((n,)),
-            dma((n,)),
-            dma((n,)),
-            dma((5,)),
-            dma((5,)),
-            dma((n,)),
             dma((n,)),
             dma(()),
+            dma(()),
+            dma((6,)),
             dma(()),
         ],
         compiler_params=pltpu.CompilerParams(

time: 79.1 us -> 76.3 us (0.965)
  Pallas kernels: 78.1 us -> 75.5 us
    pallas_call x1, Pallas kernels: 76.2 us -> 73.6 us  [body(): pl.pallas_call(functools.partial(kernel, n, tp), out_shape=(pltpu.VMEM((t...]
where the time goes in v2:
time: 76.3 us; the launch traced here: 76.1 us
  Pallas kernels  75.5 us (99%)
    pallas_call x1, Pallas kernels, body(): pl.pallas_call(functools.partial(kernel, n, tp), out_shape=(pltpu.VMEM((t...  73.6 us
    pallas_call x1, Pallas kernels, moved(): pl.pallas_call(move, out_shape=tuple((jax.ShapeDtypeStruct(a.shape, a.dty...  1.91 us

profile of v2, /device:TPU:26, one launch (start us, length us, event | category | flops | bytes accessed | tf_op | source)
XLA Modules:
  0.0 76.1 jit_solution(10277309126702865350)
XLA Ops:
  0.6 73.6 %shard_map.188 = (bf16[256,512]{1,0:T(8,128)(2,1)S(1)}, bf16[1,2048,256]{2,1,0:T(8,128)(2,1)S(1)}, bf16[1,2048,256]{2,1,0:T(8,128)(2,1)S(1)}, bf16[1,256,2048]{2...) custom-call(s32[2,256]{1,0:T(2,128)} %bitcast.2, ...), custom_call_target="tpu_custom_call" | custom-call | tf_op jit(solution)/shard_map/pallas_call | solution.py:613
  74.2 1.9 %shard_map.189 = (bf16[256,512]{1,0:T(8,128)(2,1)}, bf16[1,2048,256]{2,1,0:T(8,128)(2,1)}, bf16[1,2048,256]{2,1,0:T(8,128)(2,1)}, bf16[1,256,2048]{2,1,0:T(8,128...) custom-call(bf16[256,512]{1,0:T(8,128)(2,1)S(1)} %get-tuple-element., ...), custom_call_target="tpu_custom_call" | custom-call | tf_op jit(solution)/shard_map/pallas_call | solution.py:577

commit v3 on v2

--- a/solution.py
+++ b/solution.py
@@ -399,21 +399,37 @@
 
         experts(t)
 
-        stage_cores(t)
-
-        stage_return(t - 1)
+        @pl.when(t != 3)
+        def _():
+            stage_cores(t)
+
+        @pl.when(t == 6)
+        def _():
+            stage_cores(3)
+
+        @pl.when(t != 4)
+        def _():
+            stage_return(t - 1)
+
+        @pl.when(t == 7)
+        def _():
+            stage_return(3)
 
         @pl.when(t == 3)
         def _():
             share(t + 2)
 
-        @pl.when(jnp.logical_and(t >= 3, t < n - 3))
+        @pl.when(jnp.logical_and(t > 3, t < n - 3))
         def _():
             share(t + 3)
 
         @pl.when(t < n - 1)
         def _():
             pass_on(t + 1)
+
+        @pl.when(t == 3)
+        def _():
+            share(t + 3)
 
         return carry
 

time: 76.3 us -> 75.8 us (level)
  no operation moved by 1% of the time
where the time goes in v3:
time: 75.8 us; the launch traced here: 75.6 us
  Pallas kernels  75 us (99%)
    pallas_call x1, Pallas kernels, body(): pl.pallas_call(functools.partial(kernel, n, tp), out_shape=(pltpu.VMEM((t...  73.1 us
    pallas_call x1, Pallas kernels, moved(): pl.pallas_call(move, out_shape=tuple((jax.ShapeDtypeStruct(a.shape, a.dty...  1.91 us

profile of v3, /device:TPU:26, one launch (start us, length us, event | category | flops | bytes accessed | tf_op | source)
XLA Modules:
  0.0 75.6 jit_solution(14675707892378189125)
XLA Ops:
  0.6 73.1 %shard_map.188 = (bf16[256,512]{1,0:T(8,128)(2,1)S(1)}, bf16[1,2048,256]{2,1,0:T(8,128)(2,1)S(1)}, bf16[1,2048,256]{2,1,0:T(8,128)(2,1)S(1)}, bf16[1,256,2048]{2...) custom-call(s32[2,256]{1,0:T(2,128)} %bitcast.2, ...), custom_call_target="tpu_custom_call" | custom-call | tf_op jit(solution)/shard_map/pallas_call | solution.py:629
  73.7 1.9 %shard_map.189 = (bf16[256,512]{1,0:T(8,128)(2,1)}, bf16[1,2048,256]{2,1,0:T(8,128)(2,1)}, bf16[1,2048,256]{2,1,0:T(8,128)(2,1)}, bf16[1,256,2048]{2,1,0:T(8,128...) custom-call(bf16[256,512]{1,0:T(8,128)(2,1)S(1)} %get-tuple-element., ...), custom_call_target="tpu_custom_call" | custom-call | tf_op jit(solution)/shard_map/pallas_call | solution.py:593
